TPU v7x, 32 devices: a whole 2x2x4 slice. The times are simulated.
32 devices in a mesh: ep: 4 (over y, x), tp: 8 (over z, core).
Axes of the slice: x: 2, y: 2, z: 4, core: 2. Of those that a mesh axis runs over, the one named last changes fastest.
Arguments:
- tokens: bfloat16 [256, 4096], P(('ep', 'tp')), may hold values from -6 to 6
- rec_state: float32 [256, 2048], P('ep', 'tp'), may hold values from -40 to 40
- conv_state: bfloat16 [256, 3, 2048], P('ep', None, 'tp'), may hold values from -6 to 6
- route_ids: int32 [256, 4], P('ep'), may hold values from 0 to 15, all different within a row; in each aligned block of 8 rows (0 to 7, 8 to 15, ...) at most 2 rows name the same one
- route_weights: float32 [256, 4], P(('ep', 'tp')), may hold values from 0.1 to 1
- first_gain: bfloat16 [4096], replicated, may hold values from 0.099609375 to 1.8984375
- proj_input: bfloat16 [4096, 2048], P(None, 'tp'), may hold values from -0.09375 to 0.09375
- proj_gate: bfloat16 [4096, 2048], P(None, 'tp'), may hold values from -0.09375 to 0.09375
- conv_taps: bfloat16 [4, 2048], replicated, may hold values from -1.5 to 1.5
- decay_logit: float32 [2048], replicated, may hold values from 1 to 6
- block_decay: bfloat16 [16, 128, 128], replicated, may hold values from -0.5 to 0.5
- block_input: bfloat16 [16, 128, 128], replicated, may hold values from -0.5 to 0.5
- rec_gain: bfloat16 [2048], replicated, may hold values from 0.099609375 to 1.8984375
- proj_out: bfloat16 [2048, 4096], P('tp'), may hold values from -0.125 to 0.125
- second_gain: bfloat16 [4096], replicated, may hold values from 0.099609375 to 1.8984375
- expert_gate: bfloat16 [16, 4096, 4096], P('ep', None, 'tp'), may hold values from -0.21875 to 0.21875
- expert_up: bfloat16 [16, 4096, 4096], P('ep', None, 'tp'), may hold values from -0.21875 to 0.21875
- expert_down: bfloat16 [16, 4096, 4096], P('ep', 'tp'), may hold values from -0.0234375 to 0.0234375
Outputs:
- result: bfloat16 [256, 4096], P(('ep', 'tp'))
- new_state: float32 [256, 2048], P('ep', 'tp')
- new_conv: bfloat16 [256, 3, 2048], P('ep', None, 'tp')
Inputs may be any that keep to these rules, and one draw needn't show every extreme that they name: `route_ids`: each row names 4 different experts; in the rows of one device (aligned blocks of 8 rows) no expert is named by more than 2 rows, and one is named by exactly 2.
All inputs are finite; a program needn't handle non-finite values.
Results may differ from a plain program's by a relative error of at most 0.025.
Values may be sent and summed in bfloat16 or wider, within the bound.
A program may use at most 128 MiB of HBM per device.

v0:
```python
import jax
import jax.numpy as jnp
from jax import lax
from jax.sharding import PartitionSpec as P

EXPERTS = 16
EPS = 1e-06
CLAMP = 7.0
ALPHA = 1.702
RATE = 8.0


def norm_rows(values, gain):
    scale = lax.rsqrt(jnp.mean(values * values, axis=-1, keepdims=True) + EPS)
    return values * scale * gain.astype(jnp.float32)


def slot_positions(ids, blocks):
    rows, picks = ids.shape
    onehot = (ids[:, :, None] == jnp.arange(EXPERTS, dtype=jnp.int32)).astype(jnp.int32)
    onehot = onehot.reshape(blocks, rows // blocks * picks, EXPERTS)
    before = jnp.cumsum(onehot, axis=1) - onehot
    return jnp.sum(before * onehot, axis=-1).reshape(rows, picks)


def dispatch_rows(slots, rows_in, total):
    hits = (slots[:, :, None] == jnp.arange(total, dtype=jnp.int32)).astype(jnp.bfloat16)
    chooser = jnp.sum(hits, axis=1)
    return jnp.einsum("ns,nd->sd", chooser, rows_in, preferred_element_type=jnp.float32).astype(
        jnp.bfloat16
    )


def run_experts(piece, expert_gate, expert_up, expert_down):
    gate = jnp.einsum("erd,edf->erf", piece, expert_gate, preferred_element_type=jnp.float32)
    upper = jnp.einsum("erd,edf->erf", piece, expert_up, preferred_element_type=jnp.float32)
    clipped = jnp.minimum(gate, CLAMP)
    act = (
        (jnp.clip(upper, -CLAMP, CLAMP) + 1.0) * (clipped * jax.nn.sigmoid(ALPHA * clipped))
    ).astype(jnp.bfloat16)
    return jnp.einsum("erf,efd->erd", act, expert_down, preferred_element_type=jnp.float32)


def per_device(
    tokens,
    rec_state,
    conv_state,
    route_ids,
    route_weights,
    first_gain,
    proj_input,
    proj_gate,
    conv_taps,
    decay_logit,
    block_decay,
    block_input,
    rec_gain,
    proj_out,
    second_gain,
    expert_gate,
    expert_up,
    expert_down,
):
    tp_count = lax.axis_size("tp")
    tp_place = lax.axis_index("tp")
    local_width = proj_input.shape[1]
    seq_count = rec_state.shape[0]
    own_count = tokens.shape[0]
    top_count = route_ids.shape[1]
    capacity = max(2, own_count * top_count // EXPERTS)
    first_channel = tp_place * local_width
    own_values = tokens.astype(jnp.float32)
    normed = norm_rows(own_values, first_gain).astype(jnp.bfloat16)
    piece = lax.all_gather(normed, "tp", axis=0, tiled=True)
    both = jnp.concatenate(
        [
            jnp.dot(piece, proj_input, preferred_element_type=jnp.float32),
            jnp.dot(piece, proj_gate, preferred_element_type=jnp.float32),
        ],
        axis=1,
    )
    joined = both.astype(jnp.bfloat16)
    branch_in = joined[:, :local_width]
    branch_gate = joined[:, local_width:]
    tap_weights = lax.dynamic_slice_in_dim(conv_taps, first_channel, local_width, 1).astype(
        jnp.float32
    )
    conv_values = conv_state.astype(jnp.float32)
    conv_output = tap_weights[-1] * branch_in.astype(jnp.float32)
    for tap in range(conv_state.shape[1]):
        conv_output = conv_output + tap_weights[tap] * conv_values[:, tap]
    new_conv = jnp.concatenate([conv_state[:, 1:], branch_in[:, None, :]], axis=1)
    block_width = block_decay.shape[1]
    local_blocks = local_width // block_width
    decay_mats = lax.dynamic_slice_in_dim(block_decay, tp_place * local_blocks, local_blocks, 0)
    input_mats = lax.dynamic_slice_in_dim(block_input, tp_place * local_blocks, local_blocks, 0)
    blocked = conv_output.astype(jnp.bfloat16).reshape(seq_count, local_blocks, block_width)
    decay_gate = jax.nn.sigmoid(
        jnp.einsum("rnk,nkj->rnj", blocked, decay_mats, preferred_element_type=jnp.float32).reshape(
            seq_count, local_width
        )
    )
    input_gate = jax.nn.sigmoid(
        jnp.einsum("rnk,nkj->rnj", blocked, input_mats, preferred_element_type=jnp.float32).reshape(
            seq_count, local_width
        )
    )
    decay_logits = lax.dynamic_slice_in_dim(decay_logit, first_channel, local_width, 0)
    log_keep = -RATE * decay_gate * jax.nn.softplus(-decay_logits)
    keep_factor = jnp.exp(log_keep)
    fresh_input = jnp.sqrt(-jnp.expm1(2.0 * log_keep)) * input_gate * conv_output
    new_state = keep_factor * rec_state + fresh_input
    hidden = new_state * jax.nn.gelu(branch_gate.astype(jnp.float32))
    squares = jnp.sum(hidden * hidden, axis=1, keepdims=True)
    gain_part = lax.dynamic_slice_in_dim(rec_gain, first_channel, local_width, 0).astype(
        jnp.float32
    )
    partial_value = jnp.dot(
        (hidden * gain_part).astype(jnp.bfloat16), proj_out, preferred_element_type=jnp.float32
    )
    channels = local_width * tp_count
    width_out = proj_out.shape[1]
    own_ids = lax.dynamic_slice_in_dim(route_ids, tp_place * own_count, own_count, 0)
    own_slots = own_ids * capacity + slot_positions(own_ids, 1)
    mix_part, own_squares = (
        lax.psum_scatter(
            partial_value.astype(jnp.bfloat16), "tp", scatter_dimension=0, tiled=True
        ).astype(jnp.float32),
        lax.psum_scatter(
            squares.astype(jnp.bfloat16), "tp", scatter_dimension=0, tiled=True
        ).astype(jnp.float32),
    )
    residual = own_values + mix_part * lax.rsqrt(own_squares / channels + EPS)
    second_normed = norm_rows(residual, second_gain).astype(jnp.bfloat16)
    outgoing = dispatch_rows(own_slots, second_normed, EXPERTS * capacity).reshape(
        EXPERTS, capacity, width_out
    )
    arrived = lax.all_to_all(outgoing, "ep", split_axis=0, concat_axis=1, tiled=True)
    partials = run_experts(
        lax.all_gather(arrived, "tp", axis=1, tiled=True), expert_gate, expert_up, expert_down
    )
    summed_rows = lax.psum_scatter(
        partials.astype(jnp.bfloat16), "tp", scatter_dimension=1, tiled=True
    )
    returned = lax.all_to_all(summed_rows, "ep", split_axis=1, concat_axis=0, tiled=True)
    returned_rows = returned.reshape(EXPERTS * capacity, width_out).astype(jnp.float32)
    slot_hits = (own_slots[:, :, None] == jnp.arange(EXPERTS * capacity, dtype=jnp.int32)).astype(
        jnp.float32
    )
    combine_weights = jnp.sum(slot_hits * route_weights[:, :, None], axis=1)
    expert_mix = jnp.dot(combine_weights, returned_rows, precision=lax.Precision.HIGHEST)
    result = (residual + expert_mix).astype(jnp.bfloat16)
    return (result, new_state, new_conv)


def solution(mesh):
    in_specs = (
        P(("ep", "tp"), None),
        P("ep", "tp"),
        P("ep", None, "tp"),
        P("ep", None),
        P(("ep", "tp"), None),
        P(),
        P(None, "tp"),
        P(None, "tp"),
        P(),
        P(),
        P(),
        P(),
        P(),
        P("tp", None),
        P(),
        P("ep", None, "tp"),
        P("ep", None, "tp"),
        P("ep", "tp", None),
    )
    out_specs = (P(("ep", "tp"), None), P("ep", "tp"), P("ep", None, "tp"))
    return jax.shard_map(
        per_device, mesh=mesh, in_specs=in_specs, out_specs=out_specs, check_vma=False
    )
```

profile of v0, /device:TPU:0, one launch (start us, length us, event | category | flops | bytes accessed | tf_op | source)
XLA Modules:
  0.0 196.3 jit_solution(4809331061785495694)
XLA Ops:
  7.2 0.0 copy-start
  7.2 0.0 reduce-scatter.6.cloned.1.call-start
  7.2 0.8 dynamic-slice_convert_fusion
  8.1 0.7 convert_element_type.98
  8.8 1.0 fusion.17
  9.8 0.9 fusion.19
  10.7 16.5 %all_gather.6 = bf16[64,4096]{1,0:T(8,128)(2,1)S(1)} all-gather(bf16[8,4096]{1,0:T(8,128)(2,1)S(1)} %fusion.19), channel_id=1, replica_groups=mesh['ep'=4,'tp'=8] {'tp'}, dimensions={0}, use_global_device_ids=true | all-gather | bytes 589824 | tf_op jit(solution)/shard_map/all_gather | solution.py:74
  27.2 0.9 convert_element_type.101
  28.1 2.1 %convolution_convert_fusion.4 = bf16[64,256]{1,0:T(8,128)(2,1)S(1)} fusion(bf16[64,4096]{1,0:T(8,128)(2,1)S(1)} %all_gather.6, bf16[4096,256]{1,0:T(8,128)(2,1)} %param.24), kind=kOutput, calls=%fused_computation.22 | convolution fusion | flops 134234112 | bytes 2654208 | tf_op jit(solution)/shard_map/dot_general | solution.py:77
  30.2 1.0 fusion.11
  31.2 1.0 fusion.7
  32.2 0.8 fusion.49
  33.0 0.8 dynamic-slice_convert_fusion.2
  33.8 0.0 copy-done.6
  33.8 0.1 fusion.29
  33.9 0.0 copy-start.5
  33.9 2.2 %multiply_reduce_fusion.1 = (bf16[64]{0:T(256)(128)(2,1)S(1)}, f32[64,256]{1,0:T(8,128)S(1)}) fusion(f32[64,256]{1,0:T(8,128)S(1)} %fusion.29, bf16[64,4096]{1,0:T(8,128)(2,1)S(1)} %all_gather.6, bf16[4096,256]{1,0:T(8,128)(2,1)} %param.25), kind=kOutput, calls=%fused_computation.63 | convolution fusion | flops 134430656 | bytes 2752640 | tf_op jit(solution)/shard_map/dot_general | solution.py:78
  36.1 0.0 copy-start.8
  36.1 0.0 copy-start.7
  36.1 0.0 copy-start.10
  36.1 0.0 copy-start.3
  36.1 0.0 copy-done
  36.1 1.3 convolution_convert_fusion.1
  37.4 0.0 reduce-scatter.6.cloned.1.call-update
  37.4 0.0 all-gather.2.cloned.1.call-start
  37.5 0.1 constant_dynamic-slice_fusion
  37.6 0.1 copy.58
  37.7 0.1 eq.49
  37.7 0.1 fusion.47
  37.8 0.1 reduce_window_sum.11
  37.9 0.2 select_reduce_fusion.1
  38.1 0.1 reshape.160
  38.1 0.1 copy.50
  38.2 0.0 copy-done.10
  38.3 0.6 dynamic-slice
  39.5 17.0 %all-reduce = bf16[64,1]{0,1:T(2,128)(2,1)S(1)} all-reduce(bf16[64,1]{0,1:T(2,128)(2,1)S(1)} %bitcast.97), channel_id=3, replica_groups=mesh['ep'=4,'tp'=8] {'tp'}, use_global_device_ids=true, to_apply=%region_3.4.clone | all-reduce | flops 64 | bytes 256
  56.5 0.1 rsqrt_bitcast_fusion
  56.6 0.1 fusion.48
  56.6 13.2 %reduce-scatter.6.cloned.1.call-done = bf16[8,4096]{1,0:T(8,128)(2,1)} async-done(((bf16[64,4096]{1,0:T(8,128)(2,1)}), bf16[8,4096]{1,0:T(8,128)(2,1)}) %reduce-scatter.6.cloned.1.call-update) | async-done | bytes 65552 | tf_op jit(solution)/shard_map/reduce_scatter | solution.py:126
  69.9 1.1 multiply_reduce_fusion
  71.0 1.1 convolution_convert_fusion.2
  72.1 0.2 reshape.161
  72.3 9.2 %all_to_all.33 = bf16[16,2,4096]{2,1,0:T(2,128)(2,1)S(1)} all-to-all(bf16[16,2,4096]{2,1,0:T(2,128)(2,1)S(1)} %reshape.161), channel_id=1, replica_groups=mesh['ep'=4,'tp'=8] {'ep'}, dimensions={0} | all-to-all | bytes 524288 | tf_op jit(solution)/shard_map/all_to_all | solution.py:138
  81.5 0.2 copy.78
  81.7 0.8 all_to_all.27
  82.5 0.0 all-gather.2.cloned.1.call-update
  82.5 0.2 reduce-scatter.8.cloned.1.call-start
  82.7 26.3 %all-gather.2.cloned.1.call-done = bf16[4,64,4096]{2,1,0:T(8,128)(2,1)} async-done(((bf16[4,8,4096]{2,1,0:T(8,128)(2,1)}), bf16[4,64,4096]{2,1,0:T(8,128)(2,1)}) %all-gather.2.cloned.1.call-update) | async-done | bytes 2097168 | tf_op jit(solution)/shard_map/all_gather | solution.py:140
  109.0 9.5 %convolution_minimum_fusion = f32[4,64,512]{2,1,0:T(8,128)S(1)} fusion(bf16[4,64,4096]{2,1,0:T(8,128)(2,1)} %all-gather.2.cloned.1.call-done, bf16[4,4096,512]{2,1,0:T(8,128)(2,1)} %param.33), kind=kOutput, calls=%fused_computation.5 | convolution fusion | flops 1073872896 | bytes 19398656 | tf_op jit(solution)/shard_map/erd,edf->erf/dot_general | solution.py:35
  118.5 0.0 copy-done.2
  118.6 17.8 %convolution_convert_fusion = bf16[4,64,4096]{2,1,0:T(8,128)(2,1)} fusion(bf16[4,512,4096]{2,1,0:T(8,128)(2,1)} %param.35, bf16[4,64,4096]{2,1,0:T(8,128)(2,1)S(1)} %copy-done.2, bf16[4,4096,512]{2,1,0:T(8,128)(2,1)} %param.34, f32[4,64,512]{2,1,0:T(8,128)S(1)} %convolution_minimum_fusion), kind=kOutput, calls=%fused_computation | convolution fusion | flops 2149711872 | bytes 38273024 | tf_op jit(solution)/shard_map/erf,efd->erd/dot_general | solution.py:41
  136.4 3.2 %copy.56 = bf16[4,64,4096]{2,0,1:T(4,128)(2,1)S(1)} copy(bf16[4,64,4096]{2,1,0:T(8,128)(2,1)} %convolution_convert_fusion) | data formatting | bytes 4194304
  139.6 2.6 %copy.62 = bf16[8,8,4,4096]{3,1,2,0:T(8,128)(2,1)} copy(bf16[8,8,4,4096]{3,2,1,0:T(4,128)(2,1)S(1)} %bitcast.87) | data formatting | bytes 4194304
  142.2 0.0 reduce-scatter.8.cloned.1.call-update
  142.2 35.6 %reduce-scatter.8.cloned.1.call-done = bf16[8,16384]{1,0:T(8,128)(2,1)} async-done(((bf16[64,16384]{1,0:T(8,128)(2,1)}), bf16[8,16384]{1,0:T(8,128)(2,1)}) %reduce-scatter.8.cloned.1.call-update) | async-done | bytes 262160
  177.8 1.8 reshape.166
  179.6 3.5 %all-to-all-start.1 = ((bf16[4,8,4096]{2,0,1:T(4,128)(2,1)}), bf16[4,8,4096]{2,0,1:T(4,128)(2,1)S(1)}, u32[]{:S(2)}, u32[]{:S(2)}) async-start(bf16[4,8,4096]{2,0,1:T(4,128)(2,1)} %bitcast.19), calls=%async_computation.2 | async-start | bytes 524288 | tf_op jit(solution)/shard_map/all_to_all | solution.py:145
  183.1 0.0 slice-done
  183.1 0.7 pad_maximum_fusion
  183.8 0.1 select_reduce_fusion
  183.9 4.6 %all-to-all-done.1 = bf16[4,8,4096]{2,0,1:T(4,128)(2,1)S(1)} async-done(((bf16[4,8,4096]{2,0,1:T(4,128)(2,1)}), bf16[4,8,4096]{2,0,1:T(4,128)(2,1)S(1)}, u32[]{:S(2)}, u32[]{:S(2)}) %all-to-all-start.1) | async-done | bytes 262176 | tf_op jit(solution)/shard_map/all_to_all | solution.py:145
  188.5 0.3 copy.77
  188.8 0.1 reshape.162
  188.9 0.9 fusion
  (19 shorter events, 0.1 us)
Async XLA Ops:
  7.2 29.0 %copy-start = (bf16[256,4096]{1,0:T(8,128)(2,1)S(1)}, bf16[256,4096]{1,0:T(8,128)(2,1)}, u32[]{:S(2)}) copy-start(bf16[256,4096]{1,0:T(8,128)(2,1)} %param.31) | copy-start | bytes 6291460
  7.2 62.7 %reduce-scatter.6.cloned.1.call-start = ((), (), s32[]{:S(2)}) async-start(), calls=%async_computation.4 | async-start | bytes 589824 | tf_op jit(solution)/shard_map/reduce_scatter | solution.py:126
  27.2 6.6 %copy-start.6 = (f32[64,256]{1,0:T(8,128)S(1)}, f32[64,256]{1,0:T(8,128)}, u32[]{:S(2)}) copy-start(f32[64,256]{1,0:T(8,128)} %param.19) | copy-start | bytes 196612
  33.9 3.6 %copy-start.5 = (f32[64,256]{1,0:T(8,128)}, f32[64,256]{1,0:T(8,128)S(1)}, u32[]{:S(2)}) copy-start(f32[64,256]{1,0:T(8,128)S(1)} %fusion.29) | copy-start | bytes 196612
  36.1 1.4 copy-start.8
  36.1 2.1 %copy-start.7 = (bf16[4096]{0:T(1024)(128)(2,1)S(1)}, bf16[4096]{0:T(1024)(128)(2,1)}, u32[]{:S(2)}) copy-start(bf16[4096]{0:T(1024)(128)(2,1)} %param.32) | copy-start | bytes 24580
  36.1 2.1 %copy-start.10 = (u32[32]{0:T(128)S(1)}, u32[32]{0:T(128)}, u32[]{:S(2)}) copy-start(u32[32]{0:T(128)} %constant.63) | copy-start | bytes 388
  36.1 33.8 %copy-start.3 = (bf16[8,4096]{1,0:T(8,128)(2,1)S(1)}, bf16[8,4096]{1,0:T(8,128)(2,1)}, u32[]{:S(2)}) copy-start(bf16[8,4096]{1,0:T(8,128)(2,1)} %param.18) | copy-start | bytes 196612
  37.4 71.6 %all-gather.2.cloned.1.call-start = ((), (), s32[]{:S(2)}) async-start(), calls=%async_computation.5 | async-start | bytes 2359296 | tf_op jit(solution)/shard_map/all_gather | solution.py:140
  82.5 95.3 %reduce-scatter.8.cloned.1.call-start = ((), (), s32[]{:S(2)}) async-start(), calls=%async_computation.6 | async-start | bytes 2359296
  109.0 9.5 %copy-start.2 = (bf16[4,64,4096]{2,1,0:T(8,128)(2,1)S(1)}, bf16[4,64,4096]{2,1,0:T(8,128)(2,1)}, u32[]{:S(2)}) copy-start(bf16[4,64,4096]{2,1,0:T(8,128)(2,1)} %all-gather.2.cloned.1.call-done) | copy-start | bytes 6291460
  142.1 41.0 %slice-start = ((bf16[64,3,256]{2,0,1:T(8,128)(2,1)}), bf16[64,2,256]{2,0,1:T(8,128)(2,1)S(1)}, s32[]{:S(2)}) async-start(bf16[64,3,256]{2,0,1:T(8,128)(2,1)} %param.20), calls=%async_computation.7 | async-start | bytes 131072 | tf_op jit(solution)/shard_map/slice | solution.py:92
  142.1 41.6 %copy-start.9 = (f32[8,4]{0,1:T(4,128)S(1)}, f32[8,4]{0,1:T(4,128)}, u32[]{:S(2)}) copy-start(f32[8,4]{0,1:T(4,128)} %param.22) | copy-start | bytes 388
  142.1 47.6 %copy-start.1 = (bf16[256,4096]{1,0:T(8,128)(2,1)S(1)}, bf16[256,4096]{1,0:T(8,128)(2,1)}, u32[]{:S(2)}) copy-start(bf16[256,4096]{1,0:T(8,128)(2,1)} %param.31) | copy-start | bytes 6291460
  142.1 46.7 %copy-start.4 = (bf16[8,4096]{1,0:T(8,128)(2,1)S(1)}, bf16[8,4096]{1,0:T(8,128)(2,1)}, u32[]{:S(2)}) copy-start(bf16[8,4096]{1,0:T(8,128)(2,1)} %reduce-scatter.6.cloned.1.call-done) | copy-start | bytes 196612
  179.6 8.9 %all-to-all-start.1 = ((bf16[4,8,4096]{2,0,1:T(4,128)(2,1)}), bf16[4,8,4096]{2,0,1:T(4,128)(2,1)S(1)}, u32[]{:S(2)}, u32[]{:S(2)}) async-start(bf16[4,8,4096]{2,0,1:T(4,128)(2,1)} %bitcast.19), calls=%async_computation.2 | async-start | bytes 524288 | tf_op jit(solution)/shard_map/all_to_all | solution.py:145
Sparse Core Ops, SparseCore 0:
  37.6 32.2 reduce-scatter.5
  82.6 26.3 all-gather.1
  142.3 35.4 reduce-scatter.7
where the time goes:
time: 197 us; the launch traced here: 196 us
  waiting for transfers between devices  79.8 us (41%)
  blocking collectives  42.7 us (22%)
  matrix products  36.8 us (19%)
  between operations  14.6 us (7%)
  local copies, waits for them, and re-layouts  10.3 us (5%)
  other arithmetic  8.29 us (4%)
  starting transfers between devices  3.84 us (2%)
    unnamed x4, waiting for transfers between devices  35.6 us
    all_gather x1, waiting for transfers between devices, per_device(): lax.all_gather(arrived, 'tp', axis=1, tiled=True)  26.3 us
    dot_general x1, matrix products, run_experts(): jnp.einsum('erf,efd->erd', act, expert_down, preferred_element_type=jnp.f...  17.8 us
    unnamed x1, blocking collectives  17 us
    all_gather x1, blocking collectives, per_device(): piece = lax.all_gather(normed, 'tp', axis=0, tiled=True)  16.5 us
    reduce_scatter x1, waiting for transfers between devices, per_device(): lax.psum_scatter(partial_value.astype(jnp.bfloat16), 'tp', scatter_dimens...  13.2 us
    dot_general x1, matrix products, run_experts(): jnp.einsum('erd,edf->erf', piece, expert_gate, preferred_element_type=jnp...  9.51 us
    all_to_all x1, blocking collectives, per_device(): lax.all_to_all(outgoing, 'ep', split_axis=0, concat_axis=1, tiled=True)  9.19 us
  transfers between devices with their start and end apart: 4, of which 4 were waited for; matrix products, arithmetic and copies ran while one was open for 1% of the time, Pallas kernels for 0%

commit v1 on v0

--- a/solution.py
+++ b/solution.py
@@ -1,3 +1,4 @@
+import functools
 import jax
 import jax.numpy as jnp
 from jax import lax
@@ -8,6 +9,17 @@
 CLAMP = 7.0
 ALPHA = 1.702
 RATE = 8.0
+
+
+def stacks_all_raise(z_in, shard_axis):
+    built = tuple((z_in for _ in range(lax.axis_size(shard_axis))))
+    field_out = jnp.stack(built)
+    tile_out = lax.all_to_all(field_out, shard_axis, 0, 0)
+    mid_arr = jnp.concatenate(tile_out, axis=1)
+    return mid_arr
+
+
+match_links = functools.partial(stacks_all_raise, shard_axis="tp")
 
 
 def norm_rows(values, gain):
@@ -136,9 +148,7 @@
         EXPERTS, capacity, width_out
     )
     arrived = lax.all_to_all(outgoing, "ep", split_axis=0, concat_axis=1, tiled=True)
-    partials = run_experts(
-        lax.all_gather(arrived, "tp", axis=1, tiled=True), expert_gate, expert_up, expert_down
-    )
+    partials = run_experts(match_links(arrived), expert_gate, expert_up, expert_down)
     summed_rows = lax.psum_scatter(
         partials.astype(jnp.bfloat16), "tp", scatter_dimension=1, tiled=True
     )

time: 197 us -> 219 us (1.11)
  blocking collectives: 42.7 us -> 94.2 us
  waiting for transfers between devices: 79.8 us -> 51.5 us
    all_to_all x0 -> x1, blocking collectives: none -> 51.5 us  [stacks_all_raise(): tile_out = lax.all_to_all(field_out, shard_axis, 0, 0)]
    all_gather x1 -> x0, waiting for transfers between devices: 26.3 us -> none  [per_device(): lax.all_gather(arrived, 'tp', axis=1, tiled=True)]
    unnamed x4 -> x3, waiting for transfers between devices: 35.6 us -> 33.6 us
    unnamed x27 -> x25, local copies, waits for them, and re-layouts: 8.35 us -> 8.35 us
  transfers between devices with their start and end apart: 4 -> 3, of which waited for: 4 -> 3; matrix products, arithmetic and copies ran while one was open for 1% -> 1% of each run, Pallas kernels for 0% -> 0%
where the time goes in v1:
time: 219 us; the launch traced here: 218 us
  blocking collectives  94.2 us (43%)
  waiting for transfers between devices  51.5 us (24%)
  matrix products  36 us (16%)
  between operations  14.9 us (7%)
  local copies, waits for them, and re-layouts  9.82 us (4%)
  other arithmetic  8.29 us (4%)
  starting transfers between devices  3.6 us (2%)
    all_to_all x1, blocking collectives, stacks_all_raise(): tile_out = lax.all_to_all(field_out, shard_axis, 0, 0)  51.5 us
    unnamed x3, waiting for transfers between devices  33.6 us
    dot_general x1, matrix products, run_experts(): jnp.einsum('erf,efd->erd', act, expert_down, preferred_element_type=jnp.f...  17.8 us
    unnamed x1, blocking collectives  17 us
    all_gather x1, blocking collectives, per_device(): piece = lax.all_gather(normed, 'tp', axis=0, tiled=True)  16.5 us
    reduce_scatter x1, waiting for transfers between devices, per_device(): lax.psum_scatter(partial_value.astype(jnp.bfloat16), 'tp', scatter_dimens...  13.2 us
    all_to_all x1, blocking collectives, per_device(): lax.all_to_all(outgoing, 'ep', split_axis=0, concat_axis=1, tiled=True)  9.19 us
    dot_general x1, matrix products, run_experts(): jnp.einsum('erd,edf->erf', piece, expert_gate, preferred_element_type=jnp...  8.73 us
  transfers between devices with their start and end apart: 3, of which 3 were waited for; matrix products, arithmetic and copies ran while one was open for 1% of the time, Pallas kernels for 0%

profile of v1, /device:TPU:0, one launch (start us, length us, event | category | flops | bytes accessed | tf_op | source)
XLA Modules:
  0.0 218.3 jit_solution(18004184634365336270)
XLA Ops:
  7.2 0.0 copy-start
  7.2 0.0 reduce-scatter.6.cloned.1.call-start
  7.2 0.8 dynamic-slice_convert_fusion
  8.1 0.7 convert_element_type.98
  8.8 1.0 fusion.37
  9.8 0.9 fusion.39
  10.7 16.5 %all_gather.3 = bf16[64,4096]{1,0:T(8,128)(2,1)S(1)} all-gather(bf16[8,4096]{1,0:T(8,128)(2,1)S(1)} %fusion.39), channel_id=1, replica_groups=mesh['ep'=4,'tp'=8] {'tp'}, dimensions={0}, use_global_device_ids=true | all-gather | bytes 589824 | tf_op jit(solution)/shard_map/all_gather | solution.py:86
  27.2 0.9 convert_element_type.101
  28.1 2.1 convolution_convert_fusion.4
  30.2 1.0 fusion.25
  31.2 1.0 fusion.29
  32.2 0.8 fusion.69
  33.0 0.8 dynamic-slice_convert_fusion.2
  33.8 0.0 copy-done.5
  33.8 0.1 fusion.49
  33.9 0.0 copy-start.4
  33.9 2.2 %multiply_reduce_fusion.1 = (bf16[64]{0:T(256)(128)(2,1)S(1)}, f32[64,256]{1,0:T(8,128)S(1)}) fusion(f32[64,256]{1,0:T(8,128)S(1)} %fusion.49, bf16[64,4096]{1,0:T(8,128)(2,1)S(1)} %all_gather.3, bf16[4096,256]{1,0:T(8,128)(2,1)} %param.25), kind=kOutput, calls=%fused_computation.68 | convolution fusion | flops 134430656 | bytes 2752640 | tf_op jit(solution)/shard_map/dot_general | solution.py:90
  36.1 0.0 copy-start.7
  36.1 0.0 copy-start.6
  36.1 0.0 copy-start.9
  36.1 0.0 copy-start.2
  36.1 0.0 copy-done
  36.1 1.3 convolution_convert_fusion.1
  37.4 0.0 copy-done.4
  37.4 0.0 reduce-scatter.6.cloned.1.call-update
  37.4 0.0 reduce-scatter.8.cloned.1.call-start
  37.5 0.0 copy-done.7
  37.5 0.1 constant_dynamic-slice_fusion
  37.6 0.1 copy.70
  37.7 0.1 eq.49
  37.7 0.1 fusion.67
  37.8 0.1 reduce_window_sum.11
  37.9 0.2 select_reduce_fusion.1
  38.1 0.1 reshape.169
  38.1 0.1 copy.60
  38.2 0.0 copy-done.9
  38.3 0.6 dynamic-slice
  39.5 17.0 %all-reduce = bf16[64,1]{0,1:T(2,128)(2,1)S(1)} all-reduce(bf16[64,1]{0,1:T(2,128)(2,1)S(1)} %bitcast.120), channel_id=3, replica_groups=mesh['ep'=4,'tp'=8] {'tp'}, use_global_device_ids=true, to_apply=%region_3.4.clone | all-reduce | flops 64 | bytes 256
  56.5 0.1 rsqrt_bitcast_fusion
  56.6 0.1 fusion.68
  56.6 13.2 %reduce-scatter.6.cloned.1.call-done = bf16[8,4096]{1,0:T(8,128)(2,1)} async-done(((bf16[64,4096]{1,0:T(8,128)(2,1)}), bf16[8,4096]{1,0:T(8,128)(2,1)}) %reduce-scatter.6.cloned.1.call-update) | async-done | bytes 65552 | tf_op jit(solution)/shard_map/reduce_scatter | solution.py:138
  69.9 1.1 multiply_reduce_fusion
  71.0 1.1 convolution_convert_fusion.2
  72.1 0.2 reshape.170
  72.3 9.2 %all_to_all.35 = bf16[16,2,4096]{2,1,0:T(2,128)(2,1)S(1)} all-to-all(bf16[16,2,4096]{2,1,0:T(2,128)(2,1)S(1)} %reshape.170), channel_id=1, replica_groups=mesh['ep'=4,'tp'=8] {'ep'}, dimensions={0} | all-to-all | bytes 524288 | tf_op jit(solution)/shard_map/all_to_all | solution.py:150
  81.5 0.2 copy.61
  81.7 0.2 copy.62
  81.8 0.2 stack.5
  82.1 51.5 %all_to_all.36 = bf16[8,4,8,4096]{3,2,1,0:T(8,128)(2,1)S(1)} all-to-all(bf16[8,4,8,4096]{3,2,1,0:T(8,128)(2,1)S(1)} %stack.5), channel_id=1, replica_groups=mesh['ep'=4,'tp'=8] {'tp'}, dimensions={0} | all-to-all | bytes 4194304 | tf_op jit(solution)/shard_map/all_to_all | solution.py:17
  133.5 8.7 %fusion.16 = f32[4,64,512]{2,1,0:T(8,128)S(1)} fusion(bf16[4,4096,512]{2,1,0:T(8,128)(2,1)} %param.33, bf16[8,4,8,4096]{3,2,1,0:T(8,128)(2,1)S(1)} %all_to_all.36), kind=kOutput, calls=%fused_computation.14 | convolution fusion | flops 1073872896 | bytes 19398656 | tf_op jit(solution)/shard_map/erd,edf->erf/dot_general | solution.py:47
  142.3 17.8 %convolution_convert_fusion = bf16[4,64,4096]{2,1,0:T(8,128)(2,1)} fusion(bf16[4,512,4096]{2,1,0:T(8,128)(2,1)} %param.35, bf16[4,4096,512]{2,1,0:T(8,128)(2,1)} %param.34, f32[4,64,512]{2,1,0:T(8,128)S(1)} %fusion.16, bf16[8,4,8,4096]{3,2,1,0:T(8,128)(2,1)S(1)} %all_to_all.36), kind=kOutput, calls=%fused_computation | convolution fusion | flops 2149711872 | bytes 38273024 | tf_op jit(solution)/shard_map/erf,efd->erd/dot_general | solution.py:53
  160.1 3.2 %copy.68 = bf16[4,64,4096]{2,0,1:T(4,128)(2,1)S(1)} copy(bf16[4,64,4096]{2,1,0:T(8,128)(2,1)} %convolution_convert_fusion) | data formatting | bytes 4194304
  163.3 2.6 %copy.74 = bf16[8,8,4,4096]{3,1,2,0:T(8,128)(2,1)} copy(bf16[8,8,4,4096]{3,2,1,0:T(4,128)(2,1)S(1)} %bitcast.110) | data formatting | bytes 4194304
  165.9 0.0 reduce-scatter.8.cloned.1.call-update
  165.9 33.6 %reduce-scatter.8.cloned.1.call-done = bf16[8,16384]{1,0:T(8,128)(2,1)} async-done(((bf16[64,16384]{1,0:T(8,128)(2,1)}), bf16[8,16384]{1,0:T(8,128)(2,1)}) %reduce-scatter.8.cloned.1.call-update) | async-done | bytes 262160
  199.5 1.8 reshape.177
  201.3 3.5 %all-to-all-start.2 = ((bf16[4,8,4096]{2,0,1:T(4,128)(2,1)}), bf16[4,8,4096]{2,0,1:T(4,128)(2,1)S(1)}, u32[]{:S(2)}, u32[]{:S(2)}) async-start(bf16[4,8,4096]{2,0,1:T(4,128)(2,1)} %bitcast.22), calls=%async_computation.3 | async-start | bytes 524288 | tf_op jit(solution)/shard_map/all_to_all | solution.py:155
  204.9 0.7 pad_maximum_fusion
  205.5 0.1 select_reduce_fusion
  205.6 4.6 %all-to-all-done.2 = bf16[4,8,4096]{2,0,1:T(4,128)(2,1)S(1)} async-done(((bf16[4,8,4096]{2,0,1:T(4,128)(2,1)}), bf16[4,8,4096]{2,0,1:T(4,128)(2,1)S(1)}, u32[]{:S(2)}, u32[]{:S(2)}) %all-to-all-start.2) | async-done | bytes 262176 | tf_op jit(solution)/shard_map/all_to_all | solution.py:155
  210.2 0.3 copy.108
  210.5 0.1 reshape.173
  210.6 0.0 copy-done.3
  210.6 0.9 fusion
  (16 shorter events, 0.1 us)
Async XLA Ops:
  7.2 29.0 %copy-start = (bf16[256,4096]{1,0:T(8,128)(2,1)S(1)}, bf16[256,4096]{1,0:T(8,128)(2,1)}, u32[]{:S(2)}) copy-start(bf16[256,4096]{1,0:T(8,128)(2,1)} %param.31) | copy-start | bytes 6291460
  7.2 62.7 %reduce-scatter.6.cloned.1.call-start = ((), (), s32[]{:S(2)}) async-start(), calls=%async_computation.5 | async-start | bytes 589824 | tf_op jit(solution)/shard_map/reduce_scatter | solution.py:138
  27.2 6.6 %copy-start.5 = (f32[64,256]{1,0:T(8,128)S(1)}, f32[64,256]{1,0:T(8,128)}, u32[]{:S(2)}) copy-start(f32[64,256]{1,0:T(8,128)} %param.19) | copy-start | bytes 196612
  33.9 3.6 %copy-start.4 = (f32[64,256]{1,0:T(8,128)}, f32[64,256]{1,0:T(8,128)S(1)}, u32[]{:S(2)}) copy-start(f32[64,256]{1,0:T(8,128)S(1)} %fusion.49) | copy-start | bytes 196612
  36.1 1.4 copy-start.7
  36.1 2.1 copy-start.6
  36.1 2.1 copy-start.9
  36.1 33.8 %copy-start.2 = (bf16[8,4096]{1,0:T(8,128)(2,1)S(1)}, bf16[8,4096]{1,0:T(8,128)(2,1)}, u32[]{:S(2)}) copy-start(bf16[8,4096]{1,0:T(8,128)(2,1)} %param.18) | copy-start | bytes 196612
  37.4 162.1 %reduce-scatter.8.cloned.1.call-start = ((), (), s32[]{:S(2)}) async-start(), calls=%async_computation.6 | async-start | bytes 2359296
  165.9 39.0 %slice-start = ((bf16[64,3,256]{2,0,1:T(8,128)(2,1)}), bf16[64,2,256]{2,0,1:T(8,128)(2,1)S(1)}, s32[]{:S(2)}) async-start(bf16[64,3,256]{2,0,1:T(8,128)(2,1)} %param.20), calls=%async_computation.7 | async-start | bytes 131072 | tf_op jit(solution)/shard_map/slice | solution.py:104
  165.9 39.6 %copy-start.8 = (f32[8,4]{0,1:T(4,128)S(1)}, f32[8,4]{0,1:T(4,128)}, u32[]{:S(2)}) copy-start(f32[8,4]{0,1:T(4,128)} %param.22) | copy-start | bytes 388
  165.9 45.6 %copy-start.1 = (bf16[256,4096]{1,0:T(8,128)(2,1)S(1)}, bf16[256,4096]{1,0:T(8,128)(2,1)}, u32[]{:S(2)}) copy-start(bf16[256,4096]{1,0:T(8,128)(2,1)} %param.31) | copy-start | bytes 6291460
  165.9 44.7 %copy-start.3 = (bf16[8,4096]{1,0:T(8,128)(2,1)S(1)}, bf16[8,4096]{1,0:T(8,128)(2,1)}, u32[]{:S(2)}) copy-start(bf16[8,4096]{1,0:T(8,128)(2,1)} %reduce-scatter.6.cloned.1.call-done) | copy-start | bytes 196612
  201.3 8.9 %all-to-all-start.2 = ((bf16[4,8,4096]{2,0,1:T(4,128)(2,1)}), bf16[4,8,4096]{2,0,1:T(4,128)(2,1)S(1)}, u32[]{:S(2)}, u32[]{:S(2)}) async-start(bf16[4,8,4096]{2,0,1:T(4,128)(2,1)} %bitcast.22), calls=%async_computation.3 | async-start | bytes 524288 | tf_op jit(solution)/shard_map/all_to_all | solution.py:155
Sparse Core Ops, SparseCore 0:
  37.6 32.2 reduce-scatter.5
  166.0 33.4 reduce-scatter.7
